TPU v7x, 256 devices: a 2x2x32 block of a 4x16x32 slice. The times are simulated.
256 devices in a mesh: grp: 4 (over y, x), ep: 32 (over z), tp: 2 (over core).
Axes of the slice: x: 2, y: 2, z: 32, core: 2. Of those that a mesh axis runs over, the one named last changes fastest.
The devices are a block of a 4x16x32 slice.
Arguments:
- tokens: bfloat16 [65536, 2048], P(('grp', 'ep', 'tp')), parts along dimension 0, may hold values from -6 to 6
- norm_gain: float32 [2048], replicated, may hold values from 0.1 to 1.9
- routes: int32 [65536, 3], P(('grp', 'ep', 'tp')), parts along dimension 0, may hold values from 0 to 31, all different within a row; in each aligned block of 256 rows (0 to 255, 256 to 511, ...) at most 36 rows name the same one
- gates: float32 [65536, 3], P(('grp', 'ep', 'tp')), parts along dimension 0, may hold values from 0.2 to 1.2
- expert_gate: bfloat16 [32, 2048, 512], P('ep', None, 'tp'), may hold values from -0.125 to 0.125
- expert_up: bfloat16 [32, 2048, 512], P('ep', None, 'tp'), may hold values from -0.125 to 0.125
- expert_down: bfloat16 [32, 512, 2048], P('ep', 'tp'), may hold values from -0.25 to 0.25
- shared_gate: bfloat16 [2048, 512], replicated, may hold values from -0.125 to 0.125
- shared_up: bfloat16 [2048, 512], replicated, may hold values from -0.125 to 0.125
- shared_down: bfloat16 [512, 2048], replicated, may hold values from -0.25 to 0.25
Outputs:
- mixed: bfloat16 [65536, 2048], P(('grp', 'ep', 'tp')), parts along dimension 0
There are 4 independent parts, one for each index of `grp`. A program takes and returns all parts, laid end to end along the dimension named above; an argument that names none is the same for every part. Nothing has to cross between parts.
Inputs may be any that keep to these rules, and one draw needn't show every extreme that they name: `routes`: A row names 3 different experts. Among the rows of one device no expert is named by more than 36 rows, and in every draw some expert is named by exactly 36 rows of some device.
All inputs are finite; a program needn't handle non-finite values.
Results may differ from a plain program's by a relative error of at most 0.01.
Values may be sent and summed in bfloat16 or wider, within the bound.
A program may use at most 128 MiB of HBM per device.

v0:
```python
import jax
import jax.numpy as jnp
from jax import lax
from jax.sharding import PartitionSpec as P


def on_device(
    tokens,
    norm_gain,
    routes,
    gates,
    expert_gate,
    expert_up,
    expert_down,
    shared_gate,
    shared_up,
    shared_down,
):
    token_rows, width = tokens.shape
    top_count = routes.shape[1]
    local_experts = expert_gate.shape[0]
    groups = lax.axis_size("ep")
    experts = local_experts * groups
    capacity = 3 * token_rows * top_count // (2 * experts)
    values = tokens.astype(jnp.float32)
    scaling = lax.rsqrt(jnp.mean(values * values, axis=1, keepdims=True) + 1e-06)
    normed = (values * scaling * norm_gain[None, :]).astype(jnp.bfloat16)
    flat_routes = routes.reshape(-1)
    copies = flat_routes.shape[0]
    onehot = (flat_routes[:, None] == jnp.arange(experts, dtype=jnp.int32)[None, :]).astype(
        jnp.int32
    )
    earlier = jnp.cumsum(onehot, axis=0) - onehot
    slot_index = jnp.sum(earlier * onehot, axis=1)
    buffer_row = flat_routes * capacity + slot_index
    source_token = jnp.arange(copies, dtype=jnp.int32) // top_count
    slot_token = (
        jnp.full((experts * capacity,), token_rows, jnp.int32).at[buffer_row].set(source_token)
    )
    padded = jnp.concatenate([normed, jnp.zeros((1, width), jnp.bfloat16)], axis=0)
    outgoing = padded[slot_token].reshape(groups, local_experts, capacity, width)
    whole_gate, whole_up = (
        lax.all_gather(expert_gate, "tp", axis=2, tiled=True),
        lax.all_gather(expert_up, "tp", axis=2, tiled=True),
    )
    whole_down = lax.all_gather(expert_down, "tp", axis=1, tiled=True)
    received = lax.all_to_all(outgoing, "ep", split_axis=0, concat_axis=0, tiled=True)
    gate_values = jnp.einsum(
        "secd,edf->secf", received, whole_gate, preferred_element_type=jnp.float32
    )
    up_values = jnp.einsum("secd,edf->secf", received, whole_up, preferred_element_type=jnp.float32)
    hidden = (jax.nn.silu(gate_values) * up_values).astype(jnp.bfloat16)
    summed = jnp.einsum("secf,efd->secd", hidden, whole_down, preferred_element_type=jnp.float32)
    returned = lax.all_to_all(
        summed.astype(jnp.bfloat16), "ep", split_axis=0, concat_axis=0, tiled=True
    )
    shared_hidden = (
        jax.nn.silu(jnp.dot(normed, shared_gate, preferred_element_type=jnp.float32))
        * jnp.dot(normed, shared_up, preferred_element_type=jnp.float32)
    ).astype(jnp.bfloat16)
    shared_out = jnp.dot(shared_hidden, shared_down, preferred_element_type=jnp.float32)
    flat_back = returned.reshape(experts * capacity, width)
    picked = flat_back[buffer_row].reshape(token_rows, top_count, width)
    routed = jnp.einsum("tkd,tk->td", picked.astype(jnp.float32), gates)
    return (shared_out + routed).astype(jnp.bfloat16)


def solution(mesh):
    return jax.shard_map(
        on_device,
        mesh=mesh,
        in_specs=(
            P(("grp", "ep", "tp"), None),
            P(),
            P(("grp", "ep", "tp"), None),
            P(("grp", "ep", "tp"), None),
            P("ep", None, "tp"),
            P("ep", None, "tp"),
            P("ep", "tp", None),
            P(),
            P(),
            P(),
        ),
        out_specs=P(("grp", "ep", "tp"), None),
        check_vma=False,
    )
```

profile of v0, /device:TPU:37, one launch (start us, length us, event | category | flops | bytes accessed | tf_op | source)
XLA Modules:
  0.0 1049.7 jit_solution(6833473880233415344)
XLA Ops:
  6.6 1.0 copy.16
  7.5 0.2 eq.29
  7.7 0.2 eq.25
  7.9 0.7 broadcast_multiply_fusion
  8.7 1.7 reduce-window.6
  10.4 0.3 slice_reduce_fusion
  10.7 0.1 copy.15
  10.8 0.2 mul.61
  11.1 0.1 fusion.37
  11.2 3.4 scatter_custom_fusion
  14.6 1.5 fusion.9
  16.2 0.3 fusion.11
  16.5 1.0 copy-done.2
  17.5 5.9 gather_fusion
  23.5 7.2 reshape.85
  30.7 33.2 %all-to-all-start = ((bf16[32,1,36,2048]{3,2,1,0:T(8,128)(2,1)}), bf16[32,1,36,2048]{3,2,1,0:T(8,128)(2,1)}, u32[]{:S(2)}, u32[]{:S(2)}) async-start(bf16[32,1,36,2048]{3,2,1,0:T(8,128)(2,1)} %bitcast.105), calls=%async_computation | async-start | bytes 10485760 | tf_op jit(solution)/shard_map/all_to_all | solution.py:47
  64.0 0.7 all-gather.6.cloned.1.call-update
  64.8 0.7 all-gather.4.cloned.1.call-update
  65.6 0.7 all-gather.8.cloned.1.call-update
  66.3 29.7 %all-gather.6.cloned.1.call-done = bf16[1,2048,512]{2,1,0:T(8,128)(2,1)} async-done(((bf16[1,2048,256]{2,1,0:T(8,128)(2,1)}), bf16[1,2048,512]{2,1,0:T(8,128)(2,1)}) %all-gather.6.cloned.1.call-update) | async-done | bytes 2097168 | tf_op jit(solution)/shard_map/all_gather | solution.py:44
  96.0 417.7 %all-to-all-done = bf16[32,1,36,2048]{3,2,1,0:T(8,128)(2,1)} async-done(((bf16[32,1,36,2048]{3,2,1,0:T(8,128)(2,1)}), bf16[32,1,36,2048]{3,2,1,0:T(8,128)(2,1)}, u32[]{:S(2)}, u32[]{:S(2)}) %all-to-all-start) | async-done | bytes 4718624 | tf_op jit(solution)/shard_map/all_to_all | solution.py:47
  513.7 7.6 fusion
  521.3 11.2 %convert_bitcast_fusion = bf16[32,1,36,2048]{3,2,1,0:T(8,128)(2,1)} fusion(bf16[1,512,2048]{2,1,0:T(8,128)(2,1)} %all-gather.8.cloned.1.call-done, f32[32,36,512]{2,1,0:T(8,128)} %fusion, bf16[1,2048,512]{2,1,0:T(8,128)(2,1)} %all-gather.4.cloned.1.call-done, bf16[32,1,36,2048]{3,2,1,0:T(8,128)(2,1)} %all-to-all-done), kind=kOutput, calls=%fused_computation.7 | convolution fusion | flops 4837736448 | bytes 15990784 | tf_op jit(solution)/shard_map/secf,efd->secd/dot_general | solution.py:53
  532.5 23.2 %all-to-all-start.1 = ((bf16[32,1,36,2048]{3,2,1,0:T(8,128)(2,1)}), bf16[32,1,36,2048]{3,2,1,0:T(8,128)(2,1)}, u32[]{:S(2)}, u32[]{:S(2)}) async-start(bf16[32,1,36,2048]{3,2,1,0:T(8,128)(2,1)} %convert_bitcast_fusion), calls=%async_computation.1 | async-start | bytes 10485760 | tf_op jit(solution)/shard_map/all_to_all | solution.py:54
  555.8 0.2 copy.21
  556.0 3.1 fusion.47
  559.1 446.8 %all-to-all-done.1 = bf16[32,1,36,2048]{3,2,1,0:T(8,128)(2,1)} async-done(((bf16[32,1,36,2048]{3,2,1,0:T(8,128)(2,1)}), bf16[32,1,36,2048]{3,2,1,0:T(8,128)(2,1)}, u32[]{:S(2)}, u32[]{:S(2)}) %all-to-all-start.1) | async-done | bytes 4718624 | tf_op jit(solution)/shard_map/all_to_all | solution.py:54
  1005.9 7.2 reshape.91
  1013.1 10.1 gather_fusion.1
  1023.2 9.1 reshape.92
  1032.3 5.8 fusion.48
  1038.1 5.1 fusion.8
  (25 shorter events, 0.4 us)
Async XLA Ops:
  6.5 1031.6 %copy-start = (bf16[512,2048]{1,0:T(8,128)(2,1)S(1)}, bf16[512,2048]{1,0:T(8,128)(2,1)}, u32[]{:S(2)}) copy-start(bf16[512,2048]{1,0:T(8,128)(2,1)} %param.19) | copy-start | bytes 6291460
  6.6 9.6 copy-start.1
  6.6 9.6 copy-start.4
  16.5 1.0 copy-start.2
  30.7 483.1 %all-to-all-start = ((bf16[32,1,36,2048]{3,2,1,0:T(8,128)(2,1)}), bf16[32,1,36,2048]{3,2,1,0:T(8,128)(2,1)}, u32[]{:S(2)}, u32[]{:S(2)}) async-start(bf16[32,1,36,2048]{3,2,1,0:T(8,128)(2,1)} %bitcast.105), calls=%async_computation | async-start | bytes 10485760 | tf_op jit(solution)/shard_map/all_to_all | solution.py:47
  63.9 32.1 %all-gather.6.cloned.1.call-start = ((), (), s32[]{:S(2)}) async-start(), calls=%async_computation.3 | async-start | bytes 3145728 | tf_op jit(solution)/shard_map/all_gather | solution.py:44
  64.7 456.6 %all-gather.4.cloned.1.call-start = ((), (), s32[]{:S(2)}) async-start(), calls=%async_computation.2 | async-start | bytes 3145728 | tf_op jit(solution)/shard_map/all_gather | solution.py:43
  65.5 455.8 %all-gather.8.cloned.1.call-start = ((), (), s32[]{:S(2)}) async-start(), calls=%async_computation.4 | async-start | bytes 3145728 | tf_op jit(solution)/shard_map/all_gather | solution.py:46
  532.5 23.2 %copy-start.5 = (f32[256,3]{0,1:T(4,128)S(1)}, f32[256,3]{0,1:T(4,128)}, u32[]{:S(2)}) copy-start(f32[256,3]{0,1:T(4,128)} %param.13) | copy-start | bytes 9220
  532.5 23.4 %copy-start.3 = (bf16[256,2048]{1,0:T(8,128)(2,1)S(1)}, bf16[256,2048]{1,0:T(8,128)(2,1)}, u32[]{:S(2)}) copy-start(bf16[256,2048]{1,0:T(8,128)(2,1)} %copy-done.2) | copy-start | bytes 3145732
  532.5 473.4 %all-to-all-start.1 = ((bf16[32,1,36,2048]{3,2,1,0:T(8,128)(2,1)}), bf16[32,1,36,2048]{3,2,1,0:T(8,128)(2,1)}, u32[]{:S(2)}, u32[]{:S(2)}) async-start(bf16[32,1,36,2048]{3,2,1,0:T(8,128)(2,1)} %convert_bitcast_fusion), calls=%async_computation.1 | async-start | bytes 10485760 | tf_op jit(solution)/shard_map/all_to_all | solution.py:54
Sparse Core Ops, SparseCore 0:
  66.5 29.4 all-gather.5
  97.8 28.3 all-gather.3
  128.1 28.8 all-gather.7
where the time goes:
time: 1060 us; the launch traced here: 1050 us
  waiting for transfers between devices  896 us (85%)
  starting transfers between devices  56.6 us (5%)
  local copies, waits for them, and re-layouts  46.1 us (4%)
  matrix products  32.8 us (3%)
  between operations  13.3 us (1%)
    all_to_all x1, waiting for transfers between devices, on_device(): lax.all_to_all(summed.astype(jnp.bfloat16), 'ep', split_axis=0, concat_ax...  447 us
    all_to_all x1, waiting for transfers between devices, on_device(): lax.all_to_all(outgoing, 'ep', split_axis=0, concat_axis=0, tiled=True)  418 us
    all_to_all x1, starting transfers between devices, on_device(): lax.all_to_all(outgoing, 'ep', split_axis=0, concat_axis=0, tiled=True)  33.2 us
    all_gather x1, waiting for transfers between devices, on_device(): lax.all_gather(expert_up, 'tp', axis=2, tiled=True)  29.7 us
    all_to_all x1, starting transfers between devices, on_device(): lax.all_to_all(summed.astype(jnp.bfloat16), 'ep', split_axis=0, concat_ax...  23.2 us
  transfers between devices with their start and end apart: 5, of which 3 were waited for; matrix products, arithmetic and copies ran while one was open for 1% of the time, Pallas kernels for 0%

commit v1 on v0

v1 whole, which is shorter than its diff:
```python
import functools

import jax
import jax.numpy as jnp
from jax import lax
from jax.experimental import pallas as pl
from jax.experimental.pallas import tpu as pltpu
from jax.sharding import PartitionSpec as P

MESH = pl.DeviceIdType.MESH
BLOCK = 32


def plan(n, rows, cap):
    reach = (n // 2, n - 1 - n // 2)
    carried = []
    for far in reach:
        table = [rows]
        for hop in range(1, far + 1):
            need = cap * (far + 1 - hop)
            table.append(min(rows, -(-need // BLOCK) * BLOCK))
        carried.append(table)
    full = 1
    while all(full + 1 < len(t) and t[full + 1] == rows for t in carried):
        full += 1
    return reach, carried, full


def pieces(count, rows):
    for first in (rows // 2, rows // 4):
        if count > first:
            return ((0, first), (first, count - first))
    return ((0, count),)


def kernel(
    n, rows, cap, top,
    meta_in, rows_in, wg_in, wu_in, wd_in, out,
    x, cs, ct, wg, wu, wd, meta, g,
    in_sem, w_sem, wsend_sem, wrecv_sem,
    msend_sem, mrecv_sem, dsend_sem, drecv_sem, csend_sem, crecv_sem, out_sem,
):
    reach, carried, full = plan(n, rows, cap)
    z, core = lax.axis_index("ep"), lax.axis_index("tp")
    sign = 1 - 2 * core
    up = lax.rem(z + sign + n, n)
    down = lax.rem(z - sign + n, n)
    ahead, back = (up, down), (down, up)
    half = rows // 2
    far = reach[0]
    tail_at = []
    for d in range(2):
        at, table = 0, {}
        for hop in range(reach[d], full, -1):
            table[hop] = at
            at += carried[d][hop]
        tail_at.append(table)

    row_loads = [pltpu.make_async_copy(rows_in.at[d], x.at[d, 0], in_sem.at[d]) for d in range(2)]
    meta_loads = [pltpu.make_async_copy(meta_in.at[d], meta.at[d, 0], in_sem.at[2 + d]) for d in range(2)]
    for c in row_loads + meta_loads:
        c.start()
    w_pairs = ((wg_in, wg), (wu_in, wu), (wd_in, wd))
    w_loads = [pltpu.make_async_copy(a, b.at[0], w_sem.at[i]) for i, (a, b) in enumerate(w_pairs)]
    for c in w_loads:
        c.start()

    barrier = pltpu.get_barrier_semaphore()
    for who in ({"ep": up}, {"ep": down}, {"tp": 1 - core}):
        pl.semaphore_signal(barrier, inc=1, device_id=who, device_id_type=MESH)
    pl.semaphore_wait(barrier, 3)

    def move(d, t, q):
        start, size = q
        part = pl.ds(start, size)
        k = 0 if start == 0 else 1
        return pltpu.make_async_remote_copy(
            src_ref=x.at[d, t - 1, part], dst_ref=x.at[d, t, part],
            send_sem=dsend_sem.at[d, t, k], recv_sem=drecv_sem.at[d, t, k],
            device_id={"ep": ahead[d]}, device_id_type=MESH,
        )

    def move_meta(d, t):
        return pltpu.make_async_remote_copy(
            src_ref=meta.at[d, t - 1], dst_ref=meta.at[d, t],
            send_sem=msend_sem.at[d, t], recv_sem=mrecv_sem.at[d, t],
            device_id={"ep": ahead[d]}, device_id_type=MESH,
        )

    def weigh(d, h):
        m = meta[d, h].T
        me = z.astype(jnp.float32)
        total = jnp.zeros((rows, 1), jnp.float32)
        for k in range(top):
            total += jnp.where(m[:, k : k + 1] == me, m[:, 4 + k : 5 + k], 0.0)
        g[d, h] = total

    def expert(d, h, start, size):
        part = pl.ds(start, size)
        v = x[d, h, part, :]
        acc = None
        for s in range(2):
            a = jnp.dot(v, wg[s], preferred_element_type=jnp.float32)
            b = jnp.dot(v, wu[s], preferred_element_type=jnp.float32)
            hidden = (a * (1.0 / (1.0 + jnp.exp(-a))) * b).astype(jnp.bfloat16)
            y = jnp.dot(hidden, wd[s], preferred_element_type=jnp.float32)
            acc = y if acc is None else acc + y
        x[d, h, part, :] = (acc * g[d, h, part, :]).astype(jnp.bfloat16)

    def expert_tiles(h, lo, hi):
        size = rows // 4
        first = -(-carried[0][h] // size)

        def tile(i, carry):
            d = jnp.where(i < first, 0, 1)
            start = (i - d * first) * size
            expert(d, h, pl.multiple_of(start, size), size)
            return carry

        lax.fori_loop(lo, hi, tile, 0)

    def tile_count(h):
        size = rows // 4
        return sum(-(-carried[d][h] // size) for d in range(2) if h <= reach[d])

    for d in range(2):
        row_loads[d].wait()
        for q in pieces(carried[d][1], rows):
            move(d, 1, q).start()
        meta_loads[d].wait()
        move_meta(d, 1).start()
    w_moves = [
        pltpu.make_async_remote_copy(
            src_ref=a, dst_ref=b.at[1], send_sem=wsend_sem.at[i], recv_sem=wrecv_sem.at[i],
            device_id={"tp": 1 - core}, device_id_type=MESH,
        )
        for i, (a, b) in enumerate(w_pairs)
    ]
    for c in w_moves:
        c.start()
    for d in range(2):
        weigh(d, 0)
    for c in w_loads:
        c.wait()
    for c in w_moves:
        c.wait()

    def full_hop(t, carry):
        for k in range(2):
            q = (k * half, half)
            for d in range(2):
                if k == 0:
                    move_meta(d, t - 1).wait_recv()
                    move_meta(d, t).start()
                move(d, t - 1, q).wait_recv()
                move(d, t, q).start()
            if k == 0:
                for d in range(2):
                    weigh(d, t - 1)
            for d in range(2):
                move(d, t - 1, q).wait_send()

            def both(d, c):
                expert(d, t - 2, k * half, half)
                return c

            lax.fori_loop(0, 2, both, 0)
        return carry

    lax.fori_loop(2, full + 1, full_hop, 0)

    for t in range(full + 1, far + 1):
        h = t - 2
        count = tile_count(h)
        for k in range(2):
            for d in range(2):
                if t - 1 > reach[d]:
                    continue
                if k == 0:
                    move_meta(d, t - 1).wait_recv()
                    if t <= reach[d]:
                        move_meta(d, t).start()
                came = pieces(carried[d][t - 1], rows)
                if k < len(came):
                    move(d, t - 1, came[k]).wait_recv()
                if t <= reach[d]:
                    goes = pieces(carried[d][t], rows)
                    if k < len(goes):
                        move(d, t, goes[k]).start()
            if k == 0:
                for d in range(2):
                    if t - 1 <= reach[d]:
                        weigh(d, t - 1)
                for d in range(2):
                    for q in pieces(carried[d][t - 1], rows) if t - 1 <= reach[d] else ():
                        move(d, t - 1, q).wait_send()
            expert_tiles(h, *((0, count // 2) if k == 0 else (count // 2, count)))

    def landing(d, h):
        if isinstance(h, int) and h > full:
            return lambda start, size: ct.at[d, pl.ds(tail_at[d][h] + start, size)]
        slot = lax.rem(h - 1, 3)
        return lambda start, size: cs.at[d, slot, pl.ds(start, size)]

    def give(d, h, q):
        start, size = q
        k = 0 if start == 0 else 1
        return pltpu.make_async_remote_copy(
            src_ref=x.at[d, h, pl.ds(start, size)], dst_ref=landing(d, h)(start, size),
            send_sem=csend_sem.at[d, h, k], recv_sem=crecv_sem.at[d, h, k],
            device_id={"ep": back[d]}, device_id_type=MESH,
        )

    def add(d, h, q):
        start, size = q
        strip = 16
        at = landing(d, h + 1)(start, size)

        def one(i, carry):
            s = pl.multiple_of(i * strip, strip)
            mine = x[d, h, pl.ds(start + s, strip), :].astype(jnp.float32)
            theirs = at[pl.ds(s, strip), :].astype(jnp.float32)
            x[d, h, pl.ds(start + s, strip), :] = (mine + theirs).astype(jnp.bfloat16)
            return carry

        lax.fori_loop(0, size // strip, one, 0)

    for h in range(far, full - 1, -1):
        if h == far:
            for d in range(2):
                if far <= reach[d]:
                    for q in pieces(carried[d][far], rows):
                        move(d, far, q).wait_recv()
                    move_meta(d, far).wait_recv()
                    weigh(d, far)
            expert_tiles(far, 0, tile_count(far))
        if h == far - 1:
            for d in range(2):
                for q in pieces(carried[d][far], rows) if far <= reach[d] else ():
                    move(d, far, q).wait_send()
            expert_tiles(h, 0, tile_count(h))
        taken = [0, 0]
        for k in range(2):
            for d in range(2):
                if h > reach[d]:
                    continue
                goes = pieces(carried[d][h], rows)
                comes = pieces(carried[d][h + 1], rows) if h + 1 <= reach[d] else ()
                if k >= len(goes):
                    continue
                end = goes[k][0] + goes[k][1]
                while taken[d] < len(comes) and comes[taken[d]][0] < end:
                    q = comes[taken[d]]
                    give(d, h + 1, q).wait_recv()
                    add(d, h, q)
                    taken[d] += 1
                give(d, h, goes[k]).start()

    def full_back(i, carry):
        h = full - 1 - i
        for k in range(2):
            q = (k * half, half)
            for d in range(2):
                give(d, h + 1, q).wait_recv()
                add(d, h, q)
                give(d, h, q).start()
        return carry

    lax.fori_loop(0, full - 1, full_back, 0)

    results = []
    for k in range(2):
        q = (k * half, half)
        for d in range(2):
            give(d, 1, q).wait_recv()
            add(d, 0, q)
            part = pl.ds(k * half, half)
            results.append(pltpu.make_async_copy(x.at[d, 0, part], out.at[d, part], out_sem.at[d, k]))
            results[-1].start()

    for d in range(2):
        for h in range(full, reach[d] + 1):
            for q in pieces(carried[d][h], rows):
                give(d, h, q).wait_send()

    def drain(h, carry):
        for d in range(2):
            for k in range(2):
                give(d, h, (k * half, half)).wait_send()
        return carry

    lax.fori_loop(1, full, drain, 0)

    def drain_meta(t, carry):
        for d in range(2):
            move_meta(d, t).wait_send()
        return carry

    lax.fori_loop(1, reach[1] + 1, drain_meta, 0)
    for t in range(reach[1] + 1, far + 1):
        move_meta(0, t).wait_send()
    for c in results:
        c.wait()


def exchange(n, cap, meta, sent, w_gate, w_up, w_down):
    _, rows, width = sent.shape
    top = 3
    hidden = w_gate.shape[1]
    reach, carried, full = plan(n, rows, cap)
    slots = reach[0] + 1
    tail = max(sum(carried[d][full + 1 :]) for d in range(2))
    any_space = pl.BlockSpec(memory_space=pl.ANY)
    dma = pltpu.SemaphoreType.DMA
    return pl.pallas_call(
        functools.partial(kernel, n, rows, cap, top),
        out_shape=jax.ShapeDtypeStruct((2, rows, width), jnp.bfloat16),
        in_specs=[any_space] * 5,
        out_specs=any_space,
        scratch_shapes=[
            pltpu.VMEM((2, slots, rows, width), jnp.bfloat16),
            pltpu.VMEM((2, 3, rows, width), jnp.bfloat16),
            pltpu.VMEM((2, tail, width), jnp.bfloat16),
            pltpu.VMEM((2, width, hidden), jnp.bfloat16),
            pltpu.VMEM((2, width, hidden), jnp.bfloat16),
            pltpu.VMEM((2, hidden, width), jnp.bfloat16),
            pltpu.VMEM((2, slots, 8, rows), jnp.float32),
            pltpu.VMEM((2, slots, rows, 1), jnp.float32),
            dma((4,)),
            dma((3,)),
            dma((3,)),
            dma((3,)),
            dma((2, slots)),
            dma((2, slots)),
            dma((2, slots, 2)),
            dma((2, slots, 2)),
            dma((2, slots, 2)),
            dma((2, slots, 2)),
            dma((2, 2)),
        ],
        compiler_params=pltpu.CompilerParams(
            collective_id=0, has_side_effects=True, vmem_limit_bytes=67043328
        ),
        name="exchange",
    )(meta, sent, w_gate, w_up, w_down)


def on_device(
    tokens,
    norm_gain,
    routes,
    gates,
    expert_gate,
    expert_up,
    expert_down,
    shared_gate,
    shared_up,
    shared_down,
):
    rows, width = tokens.shape
    top = routes.shape[1]
    n = lax.axis_size("ep")
    cap = 3 * rows * top // (2 * n)
    z, core = lax.axis_index("ep"), lax.axis_index("tp")
    values = tokens.astype(jnp.float32)
    scaling = lax.rsqrt(jnp.mean(values * values, axis=1, keepdims=True) + 1e-06)
    normed = (values * scaling * norm_gain[None, :]).astype(jnp.bfloat16)

    forward = jnp.mod((routes - z) * (1 - 2 * core), n)
    first = forward <= n // 2
    distance = jnp.stack([jnp.where(first, forward, 0), jnp.where(first, 0, n - forward)])
    farthest = jnp.max(distance, axis=2)
    own = farthest[:, :, None]
    other = farthest[:, None, :]
    index = jnp.arange(rows, dtype=jnp.int32)
    before = (other > own) | ((other == own) & (index[None, None, :] < index[None, :, None]))
    rank = jnp.sum(before.astype(jnp.int32), axis=2)
    chosen = rank[:, None, :] == index[None, :, None]
    order = chosen.astype(jnp.bfloat16)
    sent = jnp.einsum("drt,tw->drw", order, normed, preferred_element_type=jnp.float32)
    sent = sent.astype(jnp.bfloat16)
    names = jnp.where(jnp.stack([first, ~first]), routes[None], -1).astype(jnp.float32)
    blank = jnp.zeros((2, rows, 4 - top), jnp.float32)
    facts = jnp.concatenate(
        [names, blank, jnp.broadcast_to(gates[None], names.shape), blank], axis=2
    )
    meta = jnp.sum(
        jnp.where(chosen[:, None, :, :], jnp.swapaxes(facts, 1, 2)[:, :, None, :], 0.0), axis=3
    )

    parts = exchange(n, cap, meta, sent, expert_gate[0], expert_up[0], expert_down[0])

    shared_hidden = (
        jax.nn.silu(jnp.dot(normed, shared_gate, preferred_element_type=jnp.float32))
        * jnp.dot(normed, shared_up, preferred_element_type=jnp.float32)
    ).astype(jnp.bfloat16)
    shared_out = jnp.dot(shared_hidden, shared_down, preferred_element_type=jnp.float32)
    routed = jnp.einsum("drt,drw->tw", order, parts, preferred_element_type=jnp.float32)
    return (shared_out + routed).astype(jnp.bfloat16)


def solution(mesh):
    return jax.shard_map(
        on_device,
        mesh=mesh,
        in_specs=(
            P(("grp", "ep", "tp"), None),
            P(),
            P(("grp", "ep", "tp"), None),
            P(("grp", "ep", "tp"), None),
            P("ep", None, "tp"),
            P("ep", None, "tp"),
            P("ep", "tp", None),
            P(),
            P(),
            P(),
        ),
        out_specs=P(("grp", "ep", "tp"), None),
        check_vma=False,
    )
```

time: 1060 us -> 640 us (0.60)
  waiting for transfers between devices: 896 us -> 0 us
  Pallas kernels: 0 us -> 616 us
  starting transfers between devices: 56.6 us -> 0 us
  local copies, waits for them, and re-layouts: 46.1 us -> 1 us
  matrix products: 32.8 us -> 12.3 us
  between operations: 13.3 us -> 0.13 us
    all_to_all x2 -> x0, waiting for transfers between devices: 864 us -> none  [the longest x1 447 us: on_device(): lax.all_to_all(summed.astype(jnp.bfloat16), 'ep', split_axis=0, concat_ax...]
    pallas_call x0 -> x1, Pallas kernels: none -> 616 us  [exchange(): pl.pallas_call(functools.partial(kernel, n, rows, cap, top), out_shape=ja...]
    all_to_all x2 -> x0, starting transfers between devices: 56.4 us -> none  [the longest x1 33.2 us: on_device(): lax.all_to_all(outgoing, 'ep', split_axis=0, concat_axis=0, tiled=True)]
    all_gather x3 -> x0, waiting for transfers between devices: 29.7 us -> none  [the longest x1 29.7 us: on_device(): lax.all_gather(expert_up, 'tp', axis=2, tiled=True)]
    reshape x3 -> x0, local copies, waits for them, and re-layouts: 23.5 us -> none  [the longest x1 9.1 us: on_device(): picked = flat_back[buffer_row].reshape(token_rows, top_count, width)]
    dot_general x3 -> x2, matrix products: 24.6 us -> 5.93 us  [the longest x1 3.43 us: on_device(): jnp.einsum('drt,tw->drw', order, normed, preferred_element_type=jnp.float32)]
    gather x2 -> x0, local copies, waits for them, and re-layouts: 16 us -> none  [the longest x1 10.1 us: on_device(): picked = flat_back[buffer_row].reshape(token_rows, top_count, width)]
  transfers between devices with their start and end apart: 5 -> 0, of which waited for: 3 -> 0; matrix products, arithmetic and copies ran while one was open for 1% -> 0% of each run, Pallas kernels for 0% -> 0%
where the time goes in v1:
time: 640 us; the launch traced here: 634 us
  Pallas kernels  616 us (96%)
  matrix products  12.3 us (2%)
    pallas_call x1, Pallas kernels, exchange(): pl.pallas_call(functools.partial(kernel, n, rows, cap, top), out_shape=ja...  616 us

profile of v1, /device:TPU:37, one launch (start us, length us, event | category | flops | bytes accessed | tf_op | source)
XLA Modules:
  0.0 634.0 jit_solution(18434666775059319002)
XLA Ops:
  0.0 0.7 select_bitcast_fusion.1
  0.7 0.7 select_convert_fusion
  1.4 0.7 broadcast_in_dim.60
  2.2 0.3 convert_reduce_fusion
  2.5 0.0 copy-start.1
  2.5 0.1 iota_compare_fusion
  2.6 0.3 copy.12
  2.9 1.2 select_reduce_fusion.meta_in
  4.2 1.5 fusion.1
  5.7 0.0 copy-start.3
  5.7 3.4 convolution_convert_fusion.rows_in
  9.1 0.0 copy-done.1
  9.1 0.0 copy-done.3
  9.1 615.9 %exchange.1 = bf16[2,256,2048]{2,1,0:T(8,128)(2,1)} custom-call(f32[2,8,256]{2,1,0:T(8,128)} %select_reduce_fusion.meta_in, bf16[2,256,2048]{2,1,0:T(8,128)(2,1)} %convolution_convert_fusion.rows_in, bf16[2048,256]{1,0:T(8,128)(2,1)} %bitcast.22, bf16[2048,256]{1,0:T(8,128)(2,1)} %bitcast.23, bf16[256,2048]{1,0:T(8,128)(2,1)} %bitcast.24), custom_call_target="tpu_custom_call" | custom-call | tf_op jit(solution)/shard_map/exchange/pallas_call | solution.py:315
  625.0 0.0 copy-start
  625.0 0.0 copy-start.2
  625.1 0.0 copy-start.4
  625.1 0.0 copy-start.5
  625.1 2.5 convolution_bitcast_fusion
  627.6 0.0 copy-done
  627.6 0.0 copy-done.2
  627.6 0.0 copy-done.4
  627.6 0.0 copy-done.5
  627.6 1.5 fusion.20
  629.2 4.8 fusion
  (7 shorter events, 0.1 us)
Async XLA Ops:
  2.5 6.6 %copy-start.1 = (s32[2,256]{1,0:T(2,128)}, s32[2,256]{1,0:T(2,128)S(1)}, u32[]{:S(2)}) copy-start(s32[2,256]{1,0:T(2,128)S(1)} %convert_reduce_fusion) | copy-start | bytes 6148
  5.7 3.4 copy-start.3
  625.0 2.6 copy-start
  625.0 2.6 copy-start.2
  625.1 2.5 copy-start.4
  625.1 2.5 copy-start.5
